TPU v7x, 256 devices: a whole 4x4x8 slice. The times are simulated.
256 devices in a mesh: sp: 64 (over z, y, core), tp: 4 (over x).
Axes of the slice: x: 4, y: 4, z: 8, core: 2. Of those that a mesh axis runs over, the one named last changes fastest.
Arguments:
- stream_in: bfloat16 [49152, 2048], P(('sp', 'tp')), may hold values from -6 to 6
- query_wide: bfloat16 [49152, 512], P('sp', 'tp'), may hold values from -6 to 6
- key_wide: bfloat16 [49152, 512], P('sp', 'tp'), may hold values from -6 to 6
- value_wide: bfloat16 [49152, 512], P('sp', 'tp'), may hold values from -6 to 6
- gate_wide: bfloat16 [49152, 512], P('sp', 'tp'), may hold values from -6 to 6
- decay_wide: float32 [4, 49152], P('tp', 'sp'), may hold values from -2.3 to 0, as said below
- query_narrow: bfloat16 [49152, 512], P('sp', 'tp'), may hold values from -6 to 6
- key_narrow: bfloat16 [49152, 512], P('sp', 'tp'), may hold values from -6 to 6
- value_narrow: bfloat16 [49152, 512], P('sp', 'tp'), may hold values from -6 to 6
- gate_narrow: bfloat16 [49152, 512], P('sp', 'tp'), may hold values from -6 to 6
- decay_narrow: float32 [8, 49152], P('tp', 'sp'), may hold values from -2.3 to 0, as said below
- output_wide: bfloat16 [512, 2048], P('tp'), may hold values from -0.25 to 0.25
- output_narrow: bfloat16 [512, 2048], P('tp'), may hold values from -0.25 to 0.25
- norm_gain: bfloat16 [2048], replicated, may hold values from 0.099609375 to 1.8984375
- up_weight: bfloat16 [2048, 8192], P('sp', 'tp'), may hold values from -0.125 to 0.125
- down_weight: bfloat16 [8192, 2048], P('tp', 'sp'), may hold values from -0.0625 to 0.0625
Outputs:
- layer_out: bfloat16 [49152, 2048], P(('sp', 'tp'))
Inputs may be any that keep to these rules, and one draw needn't show every extreme that they name: `decay_wide`: each entry is the logarithm of one head's retention factor at one position. `decay_narrow`: each entry is the logarithm of one head's retention factor at one position.
All inputs are finite; a program needn't handle non-finite values.
Results may differ from a plain program's by a relative error of at most 0.02.
Values may be sent and summed in bfloat16 or wider, within the bound.
A program may use at most 128 MiB of HBM per device.

v0:
```python
import jax
import jax.numpy as jnp
from jax import lax
from jax.sharding import Mesh
from jax.sharding import PartitionSpec as P

HDW = 128
HDN = 64
BLOCK = 128
SP = ("sp_0", "sp_1", "sp_2")
SP_TP = ("sp_0", "sp_1", "sp_2", "tp")
head_eps = 1e-05
norm_eps = 1e-06
rope_base = 10000.0


def rows_first(arrays, axis, dims):
    turned = [jnp.moveaxis(a, dim, 0) for a, dim in zip(arrays, dims)]
    both = jnp.concatenate([t.reshape(len(t), -1) for t in turned], axis=1)
    out, at, finished = (lax.all_gather(both, axis, axis=0, tiled=True), 0, [])
    for t, dim in zip(turned, dims):
        section = out[:, at : at + t[0].size].reshape(-1, *t.shape[1:])
        finished.append(jnp.moveaxis(section, 0, dim))
        at += t[0].size
    return tuple(finished)


def nothing_yet(shard, identity):
    return jax.tree.map(
        lambda part, zero: jnp.zeros_like(part) + jnp.asarray(zero, part.dtype), shard, identity
    )


def gathered_once(shard, axis):
    leaves = jax.tree.leaves(shard)
    sequence = sorted(range(len(leaves)), key=lambda k: -leaves[k].size)
    width = (1, *leaves[sequence[0]].shape)[-1]
    lines = [
        jnp.pad(leaves[k].reshape(-1), (0, -leaves[k].size % width)).reshape(-1, width)
        for k in sequence
    ]
    both, at, found = (lax.all_gather(jnp.concatenate(lines), axis), 0, {})
    for k, line in zip(sequence, lines):
        section = both[:, at : at + len(line)].reshape(len(both), -1)
        found[k] = section[:, : leaves[k].size].reshape(-1, *leaves[k].shape)
        at += len(line)
    numbers = iter(range(len(leaves)))
    return jax.tree.map(lambda _: found[next(numbers)], shard)


def entering(shard, axes, combine, identity):
    before = start = nothing_yet(shard, identity)
    so_far = shard
    for axis in reversed(axes):
        length, mine = (lax.axis_size(axis), lax.axis_index(axis))
        pieces = gathered_once(
            jax.tree.map(
                lambda part, kind: part.astype(kind),
                so_far,
                (jnp.bfloat16, jnp.bfloat16, jnp.bfloat16, jnp.bfloat16),
            ),
            axis,
        )
        inside, so_far = (start, start)
        for k in range(length):
            passed = k < mine
            so_far = combine(
                so_far, jax.tree.map(lambda part, own: part[k].astype(own.dtype), pieces, shard)
            )
            inside = jax.tree.map(lambda new, old: jnp.where(passed, new, old), so_far, inside)
        before = combine(inside, before)
    return before


def in_blocks(shard, dim, length):
    before, after = (shard.shape[:dim], shard.shape[dim + 1 :])
    return jnp.moveaxis(shard.reshape(*before, length, -1, *after), dim, 0)


def sum_at_owner(shard, axis, dim):
    tiles = in_blocks(shard, dim, lax.axis_size(axis))
    arrived = lax.all_to_all(tiles, axis, split_axis=0, concat_axis=0, tiled=True)
    return arrived.astype(jnp.float32).sum(axis=0)


def rotate(values, places):
    half = values.shape[-1] // 2
    inverse = rope_base ** (-jnp.arange(half, dtype=jnp.float32) / half)
    angles = places[:, None] * inverse[None, :]
    cosine = jnp.cos(angles)[:, None, :]
    sine = jnp.sin(angles)[:, None, :]
    front = values[..., :half]
    back = values[..., half:]
    return jnp.concatenate([front * cosine - back * sine, back * cosine + front * sine], axis=-1)


def block_step(carried, inputs):
    query, keys, values, log_rate = inputs
    running = jnp.cumsum(log_rate, axis=0)
    spread = running[:, None, :] - running[None, :, :]
    length = log_rate.shape[0]
    lower = (jnp.arange(length)[:, None] >= jnp.arange(length)[None, :])[:, :, None]
    factor = jnp.where(lower, jnp.exp(jnp.minimum(spread, 0.0)), 0.0)
    scores = jnp.einsum("thd,shd->tsh", query, keys) * factor
    within = jnp.einsum("tsh,she->the", scores, values)
    across = jnp.einsum("thd,hde->the", query, carried) * jnp.exp(running)[:, :, None]
    tail_decay = jnp.exp(running[-1][None, :] - running)
    updated = jnp.exp(running[-1])[:, None, None] * carried + jnp.einsum(
        "shd,she->hde", keys * tail_decay[:, :, None], values
    )
    return (updated, within + across)


def head_norm(values):
    centre = values - jnp.mean(values, axis=-1, keepdims=True)
    spread = jnp.mean(centre * centre, axis=-1, keepdims=True)
    return centre * lax.rsqrt(spread + head_eps)


def local_group(query, keys, values, log_rate, width, places):
    length = query.shape[0]
    count_of_heads = query.shape[1] // width
    blocks = length // BLOCK

    def split(array):
        return array.astype(jnp.float32).reshape(length, count_of_heads, width)

    query_rot = rotate(split(query), places)
    keys_rot = rotate(split(keys), places) * width ** (-0.5)
    rates = log_rate.T
    carried = jnp.zeros((count_of_heads, width, width), jnp.float32)
    final_state, outputs = lax.scan(
        block_step,
        carried,
        (
            query_rot.reshape(blocks, BLOCK, count_of_heads, width),
            keys_rot.reshape(blocks, BLOCK, count_of_heads, width),
            split(values).reshape(blocks, BLOCK, count_of_heads, width),
            rates.reshape(blocks, BLOCK, count_of_heads),
        ),
    )
    running = jnp.cumsum(rates, axis=0)
    return (
        query_rot,
        outputs.reshape(length, count_of_heads, width),
        final_state,
        jnp.exp(running[-1]),
        running,
    )


def finish_group(query_rot, outputs, incoming, running, gate):
    length = outputs.shape[0]
    outputs = (
        outputs + jnp.einsum("thd,hde->the", query_rot, incoming) * jnp.exp(running)[:, :, None]
    )
    normed = head_norm(outputs).reshape(length, -1)
    return (jax.nn.silu(gate.astype(jnp.float32)) * normed).astype(jnp.bfloat16)


def chain(earlier, later):
    rate_wide, memory_wide, rate_narrow, memory_narrow = earlier
    later_rate_wide, later_memory_wide, later_rate_narrow, later_memory_narrow = later
    return (
        rate_wide * later_rate_wide,
        memory_wide * later_rate_wide[:, None, None] + later_memory_wide,
        rate_narrow * later_rate_narrow,
        memory_narrow * later_rate_narrow[:, None, None] + later_memory_narrow,
    )


def row_norm(middle, norm_gain):
    middle_f = middle.astype(jnp.float32)
    scale = lax.rsqrt(jnp.mean(middle_f * middle_f, axis=-1, keepdims=True) + norm_eps)
    return (middle_f * scale * norm_gain.astype(jnp.float32)).astype(jnp.bfloat16)


def on_device(
    stream_in,
    query_wide,
    key_wide,
    value_wide,
    gate_wide,
    decay_wide,
    query_narrow,
    key_narrow,
    value_narrow,
    gate_narrow,
    decay_narrow,
    output_wide,
    output_narrow,
    norm_gain,
    up_weight,
    down_weight,
):
    length = query_wide.shape[0]
    up_full, down_full = rows_first((up_weight, down_weight), SP, (0, 1))
    places = (lax.axis_index(SP) * length + jnp.arange(length, dtype=jnp.int32)).astype(jnp.float32)
    wide_query, wide_out, wide_state, wide_total, wide_running = local_group(
        query_wide, key_wide, value_wide, decay_wide, HDW, places
    )
    narrow_query, narrow_out, narrow_state, narrow_total, narrow_running = local_group(
        query_narrow, key_narrow, value_narrow, decay_narrow, HDN, places
    )
    identity = (
        jnp.ones_like(wide_total),
        jnp.zeros_like(wide_state),
        jnp.ones_like(narrow_total),
        jnp.zeros_like(narrow_state),
    )
    incoming = entering((wide_total, wide_state, narrow_total, narrow_state), SP, chain, identity)
    mixed_wide = finish_group(wide_query, wide_out, incoming[1], wide_running, gate_wide)
    mixed_narrow = finish_group(narrow_query, narrow_out, incoming[3], narrow_running, gate_narrow)
    mixed_sum = sum_at_owner(
        (
            jnp.dot(mixed_wide, output_wide, preferred_element_type=jnp.float32)
            + jnp.dot(mixed_narrow, output_narrow, preferred_element_type=jnp.float32)
        ).astype(jnp.bfloat16),
        "tp",
        0,
    )
    middle = (stream_in.astype(jnp.float32) + mixed_sum).astype(jnp.bfloat16)
    normed = lax.all_gather(row_norm(middle, norm_gain), "tp", axis=0, tiled=True)
    up_sum = jnp.dot(normed, up_full, preferred_element_type=jnp.float32)
    hidden = jnp.square(jax.nn.relu(up_sum)).astype(jnp.bfloat16)
    down_sum = jnp.dot(hidden, down_full, preferred_element_type=jnp.float32)
    down_rows = lax.psum_scatter(
        down_sum.astype(jnp.bfloat16), "tp", scatter_dimension=0, tiled=True
    ).astype(jnp.float32)
    return (middle.astype(jnp.float32) + down_rows).astype(jnp.bfloat16)


def solution(mesh):
    split = Mesh(mesh.devices.reshape(8, 4, 2, mesh.shape["tp"]), ("sp_0", "sp_1", "sp_2", "tp"))
    in_specs = (
        P(SP_TP, None),
        P(SP, "tp"),
        P(SP, "tp"),
        P(SP, "tp"),
        P(SP, "tp"),
        P("tp", SP),
        P(SP, "tp"),
        P(SP, "tp"),
        P(SP, "tp"),
        P(SP, "tp"),
        P("tp", SP),
        P("tp", None),
        P("tp", None),
        P(),
        P(SP, "tp"),
        P("tp", SP),
    )
    out_specs = P(SP_TP, None)
    return jax.shard_map(
        on_device, mesh=split, in_specs=in_specs, out_specs=out_specs, check_vma=False
    )
```

profile of v0, /device:TPU:1, one launch (start us, length us, event | category | flops | bytes accessed | tf_op | source)
XLA Modules:
  0.0 398.5 jit_solution(7533716243381743910)
XLA Ops:
  6.6 1.1 copy.156
  7.8 1.1 copy.158
  10.4 25.0 %while.27 = (s32[]{:T(128)}, f32[2,64,64]{2,1,0:T(8,128)S(1)}, f32[6,128,2,64]{1,0,3,2:T(8,128)}, f32[6,128,2]{2,1,0:T(8,128)S(1)}, f32[6,128,2,64]{1,0,3,2:T(8,...) while((s32[]{:T(128)}, f32[2,64,64]{2,1,0:T(8,128)S(1)}, ...), condition=%wide.region_5.6_spmd.clone, body=%wide.region_3.5_spmd.clone.sunk | while | flops 12877827 | bytes 1099440 | solution.py:132
  11.5 2.8 dynamic_update_slice.14
  15.7 2.8 dynamic_update_slice.14
  19.9 2.8 dynamic_update_slice.14
  24.0 2.8 dynamic_update_slice.14
  28.2 2.8 dynamic_update_slice.14
  32.3 2.8 dynamic_update_slice.14
  35.5 1.0 reshape_reshape.22
  36.5 1.9 fusion.88
  38.6 0.9 maximum_multiply_fusion.1
  39.5 22.9 %while.26 = (s32[]{:T(128)}, f32[1,128,128]{2,1,0:T(8,128)S(1)}, f32[6,128,1,128]{3,1,0,2:T(8,128)}, f32[6,128,1]{1,2,0:T(1,128)S(1)}, f32[6,128,1,128]{3,2,1,0:...) while((s32[]{:T(128)}, f32[1,128,128]{2,1,0:T(8,128)S(1)}, ...), condition=%wide.region_2.3_spmd.clone, body=%wide.region_0.2_spmd.clone.sunk | while | flops 17006596 | bytes 1515172 | solution.py:132
  40.5 0.6 fusion.342
  41.9 0.6 constant_dynamic-update-slice_fusion.2
  44.3 0.6 fusion.342
  45.7 0.6 constant_dynamic-update-slice_fusion.2
  49.6 0.6 constant_dynamic-update-slice_fusion.2
  53.4 0.6 constant_dynamic-update-slice_fusion.2
  57.2 0.6 constant_dynamic-update-slice_fusion.2
  61.0 0.6 constant_dynamic-update-slice_fusion.2
  63.2 0.6 slice.432
  63.8 0.7 slice.431
  65.8 0.6 reduce-window.14
  67.1 4.7 %all-gather.3 = bf16[2,194,128]{2,1,0:T(8,128)(2,1)S(1)} all-gather(bf16[1,194,128]{2,1,0:T(8,128)(2,1)S(1)} %maximum_bitcast_fusion), channel_id=2, replica_groups=mesh['sp_0'=8,'sp_1'=4,'sp_2'=2,'tp'=4] {'sp_2'}, dimensions={0}, use_global_device_ids=true | all-gather | bytes 148992 | tf_op jit(solution)/shard_map/all_gather | solution.py:42
  74.8 9.3 %all-gather.4 = bf16[4,194,128]{2,1,0:T(8,128)(2,1)S(1)} all-gather(bf16[1,194,128]{2,1,0:T(8,128)(2,1)S(1)} %maximum_bitcast_fusion.1), channel_id=3, replica_groups=mesh['sp_0'=8,'sp_1'=4,'sp_2'=2,'tp'=4] {'sp_1'}, dimensions={0}, use_global_device_ids=true | all-gather | bytes 248320 | tf_op jit(solution)/shard_map/all_gather | solution.py:42
  87.2 0.6 fusion.271
  89.2 21.5 %all-gather.5 = bf16[8,194,128]{2,1,0:T(8,128)(2,1)S(1)} all-gather(bf16[1,194,128]{2,1,0:T(8,128)(2,1)S(1)} %maximum_bitcast_fusion.2), channel_id=4, replica_groups=mesh['sp_0'=8,'sp_1'=4,'sp_2'=2,'tp'=4] {'sp_0'}, dimensions={0}, use_global_device_ids=true | all-gather | bytes 446976 | tf_op jit(solution)/shard_map/all_gather | solution.py:42
  110.7 0.6 bitcast_convert_fusion.8
  111.9 0.6 slice_convert_fusion.11
  112.5 0.7 fusion.269
  113.8 0.7 copy.176
  114.5 0.7 copy.177
  115.3 0.7 copy.178
  116.1 0.7 copy.179
  116.9 0.7 copy.180
  117.6 0.8 reshape.1118
  118.4 0.7 copy.181
  119.1 0.8 reshape.1119
  119.9 0.7 copy.182
  120.6 0.8 reshape.1120
  121.5 0.7 copy.183
  122.2 0.8 reshape.1121
  123.0 0.7 copy.184
  123.8 0.7 copy.185
  124.6 0.7 copy.186
  125.4 1.6 fusion.292
  127.1 1.1 copy.170
  128.2 0.6 fusion.288
  134.7 1.2 copy.169
  136.6 1.2 fusion.291
  137.8 1.1 copy.153
  139.1 1.0 fusion.93
  140.1 2.7 add_convert_fusion
  142.8 4.8 %all-to-all-start = ((bf16[4,192,2048]{2,1,0:T(8,128)(2,1)}), bf16[4,192,2048]{2,1,0:T(8,128)(2,1)}, u32[]{:S(2)}, u32[]{:S(2)}) async-start(bf16[4,192,2048]{2,1,0:T(8,128)(2,1)} %bitcast.454), calls=%async_computation | async-start | bytes 6291456 | tf_op jit(solution)/shard_map/all_to_all | solution.py:82
  147.8 27.9 %all-to-all-done = bf16[4,192,2048]{2,1,0:T(8,128)(2,1)} async-done(((bf16[4,192,2048]{2,1,0:T(8,128)(2,1)}), bf16[4,192,2048]{2,1,0:T(8,128)(2,1)}, u32[]{:S(2)}, u32[]{:S(2)}) %all-to-all-start) | async-done | bytes 3145760 | tf_op jit(solution)/shard_map/all_to_all | solution.py:82
  175.8 2.7 convert_reduce_fusion
  178.8 1.1 fusion.63
  180.1 0.7 pad_maximum_fusion.2
  180.9 47.7 %all-gather.9.cloned.1.call-done = bf16[768,2048]{1,0:T(8,128)(2,1)} async-done(((bf16[192,2048]{1,0:T(8,128)(2,1)}), bf16[768,2048]{1,0:T(8,128)(2,1)}) %all-gather.9.cloned.1.call-update) | async-done | bytes 3145744 | tf_op jit(solution)/shard_map/all_gather | solution.py:223
  228.6 102.9 %all-gather.11.cloned.1.call-done = bf16[2048,4096]{1,0:T(8,128)(2,1)} async-done(((bf16[32,4096]{1,0:T(8,128)(2,1)}), bf16[2048,4096]{1,0:T(8,128)(2,1)}) %all-gather.11.cloned.1.call-update) | async-done | bytes 16777232 | tf_op jit(solution)/shard_map/all_gather | solution.py:20
  331.5 20.7 %fusion.55 = bf16[768,2048]{1,0:T(8,128)(2,1)} fusion(bf16[2048,4096]{1,0:T(8,128)(2,1)} %all-gather.11.cloned.1.call-done, bf16[768,2048]{1,0:T(8,128)(2,1)} %all-gather.9.cloned.1.call-done), kind=kOutput, calls=%fused_computation.75 | convolution fusion | flops 12891193344 | bytes 23068672 | tf_op jit(solution)/shard_map/dot_general | solution.py:226
  352.2 37.5 %reduce-scatter.2.cloned.1.call-done = bf16[192,2048]{1,0:T(8,128)(2,1)} async-done(((bf16[768,2048]{1,0:T(8,128)(2,1)}), bf16[192,2048]{1,0:T(8,128)(2,1)}) %reduce-scatter.2.cloned.1.call-update) | async-done | bytes 786448 | tf_op jit(solution)/shard_map/reduce_scatter | solution.py:227
  389.7 2.3 fusion.64
  (288 shorter events, 29.7 us)
Async XLA Ops:
  6.5 132.5 %copy-start = (bf16[128,2048]{1,0:T(8,128)(2,1)S(1)}, bf16[128,2048]{1,0:T(8,128)(2,1)}, u32[]{:S(2)}) copy-start(bf16[128,2048]{1,0:T(8,128)(2,1)} %param.31) | copy-start | bytes 1572868
  6.5 3.0 copy-start.6
  7.8 2.3 copy-start.9
  10.4 26.1 %copy-start.4 = (bf16[768,128]{1,0:T(8,128)(2,1)S(1)}, bf16[768,128]{1,0:T(8,128)(2,1)}, u32[]{:S(2)}) copy-start(bf16[768,128]{1,0:T(8,128)(2,1)} %param.21) | copy-start | bytes 589828
  10.4 26.0 %copy-start.5 = (bf16[768,128]{1,0:T(8,128)(2,1)S(1)}, bf16[768,128]{1,0:T(8,128)(2,1)}, u32[]{:S(2)}) copy-start(bf16[768,128]{1,0:T(8,128)(2,1)} %param.22) | copy-start | bytes 589828
  36.5 3.0 copy-start.14
  71.8 15.4 %copy-start.15 = (f32[2]{0:T(128)}, f32[2]{0:T(128)S(1)}, u32[]{:S(2)}) copy-start(f32[2]{0:T(128)S(1)} %bitcast_convert_fusion.12) | copy-start | bytes 28
  73.3 52.0 %copy-start.3 = (f32[6,128,2,64]{1,0,3,2:T(8,128)S(1)}, f32[6,128,2,64]{1,0,3,2:T(8,128)}, u32[]{:S(2)}) copy-start(f32[6,128,2,64]{1,0,3,2:T(8,128)} %get-tuple-element.84) | copy-start | bytes 1179652
  87.2 0.9 copy-start.12
  87.2 1.1 copy-start.11
  87.2 23.5 %copy-start.10 = (f32[2]{0:T(128)}, f32[2]{0:T(128)S(1)}, u32[]{:S(2)}) copy-start(f32[2]{0:T(128)S(1)} %get-tuple-element.255) | copy-start | bytes 28
  139.0 1.1 copy-start.2
  142.8 5.0 %copy-start.13 = (bf16[2048]{0:T(1024)(128)(2,1)S(1)}, bf16[2048]{0:T(1024)(128)(2,1)}, u32[]{:S(2)}) copy-start(bf16[2048]{0:T(1024)(128)(2,1)} %param.33) | copy-start | bytes 12292
  142.8 33.0 %all-to-all-start = ((bf16[4,192,2048]{2,1,0:T(8,128)(2,1)}), bf16[4,192,2048]{2,1,0:T(8,128)(2,1)}, u32[]{:S(2)}, u32[]{:S(2)}) async-start(bf16[4,192,2048]{2,1,0:T(8,128)(2,1)} %bitcast.454), calls=%async_computation | async-start | bytes 6291456 | tf_op jit(solution)/shard_map/all_to_all | solution.py:82
  147.6 30.9 %copy-start.1 = (bf16[192,2048]{1,0:T(8,128)(2,1)S(1)}, bf16[192,2048]{1,0:T(8,128)(2,1)}, u32[]{:S(2)}) copy-start(bf16[192,2048]{1,0:T(8,128)(2,1)} %param.20) | copy-start | bytes 2359300
  147.6 81.0 %all-gather.9.cloned.1.call-start = ((), (), s32[]{:S(2)}) async-start(), calls=%async_computation.2 | async-start | bytes 3932160 | tf_op jit(solution)/shard_map/all_gather | solution.py:223
  178.5 1.6 copy-start.7
  178.5 1.6 copy-start.8
  180.0 151.5 %all-gather.11.cloned.1.call-start = ((), (), s32[]{:S(2)}) async-start(), calls=%async_computation.3 | async-start | bytes 17039360 | tf_op jit(solution)/shard_map/all_gather | solution.py:20
  180.8 208.9 %reduce-scatter.2.cloned.1.call-start = ((), (), s32[]{:S(2)}) async-start(), calls=%async_computation.4 | async-start | bytes 3932160 | tf_op jit(solution)/shard_map/reduce_scatter | solution.py:227
Sparse Core Ops, SparseCore 0:
  180.1 48.4 all-gather.8
  231.4 100.0 all-gather.10
  352.4 37.3 reduce-scatter.1
where the time goes:
time: 400 us; the launch traced here: 399 us
  waiting for transfers between devices  216 us (54%)
  local copies, waits for them, and re-layouts  50.2 us (13%)
  matrix products  35.7 us (9%)
  blocking collectives  35.5 us (9%)
  between operations  26.9 us (7%)
  other arithmetic  24.5 us (6%)
  starting transfers between devices  5.08 us (1%)
  loops' own time  4.6 us (1%)
    all_gather x1, waiting for transfers between devices, rows_first(): out, at, finished = (lax.all_gather(both, axis, axis=0, tiled=True), 0, [])  103 us
    all_gather x1, waiting for transfers between devices, on_device(): lax.all_gather(row_norm(middle, norm_gain), 'tp', axis=0, tiled=True)  47.7 us
    reduce_scatter x1, waiting for transfers between devices, on_device(): lax.psum_scatter(down_sum.astype(jnp.bfloat16), 'tp', scatter_dimension=0...  37.5 us
    all_gather x3, blocking collectives, gathered_once(): both, at, found = (lax.all_gather(jnp.concatenate(lines), axis), 0, {})  35.5 us
    all_to_all x1, waiting for transfers between devices, sum_at_owner(): lax.all_to_all(tiles, axis, split_axis=0, concat_axis=0, tiled=True)  27.9 us
    dynamic_update_slice x18, local copies, waits for them, and re-layouts, local_group(): lax.scan(block_step, carried, (query_rot.reshape(blocks, BLOCK, count_of_...  21.1 us
    dot_general x1, matrix products, on_device(): down_sum = jnp.dot(hidden, down_full, preferred_element_type=jnp.float32)  20.7 us
    convert_element_type x28, local copies, waits for them, and re-layouts, entering(): part[k].astype(own.dtype)  12.1 us
  transfers between devices with their start and end apart: 4, of which 4 were waited for; matrix products, arithmetic and copies ran while one was open for 0% of the time, Pallas kernels for 0%

commit v1 on v0

--- a/solution.py
+++ b/solution.py
@@ -12,6 +12,19 @@
 head_eps = 1e-05
 norm_eps = 1e-06
 rope_base = 10000.0
+
+
+def ring_gather(array, axis, dim):
+    ways = lax.axis_size(axis)
+    up = [(d, (d + 1) % ways) for d in range(ways)]
+    down = [(d, (d - 1) % ways) for d in range(ways)]
+    earlier, later = ([array], [array])
+    for _ in range(ways // 2):
+        earlier.append(lax.ppermute(earlier[-1], axis, up))
+    for _ in range((ways - 1) // 2):
+        later.append(lax.ppermute(later[-1], axis, down))
+    line = jnp.concatenate([*earlier[::-1], *later[1:]], axis=dim)
+    return jnp.roll(line, (lax.axis_index(axis) - ways // 2) * array.shape[dim], axis=dim)
 
 
 def rows_first(arrays, axis, dims):
@@ -220,7 +233,7 @@
         0,
     )
     middle = (stream_in.astype(jnp.float32) + mixed_sum).astype(jnp.bfloat16)
-    normed = lax.all_gather(row_norm(middle, norm_gain), "tp", axis=0, tiled=True)
+    normed = ring_gather(row_norm(middle, norm_gain), "tp", 0)
     up_sum = jnp.dot(normed, up_full, preferred_element_type=jnp.float32)
     hidden = jnp.square(jax.nn.relu(up_sum)).astype(jnp.bfloat16)
     down_sum = jnp.dot(hidden, down_full, preferred_element_type=jnp.float32)

time: 400 us -> 305 us (0.76)
  waiting for transfers between devices: 216 us -> 103 us
  local copies, waits for them, and re-layouts: 50.2 us -> 57.5 us
  blocking collectives: 35.5 us -> 40.2 us
    all_gather x1, waiting for transfers between devices: 103 us -> 0.01 us  [rows_first(): out, at, finished = (lax.all_gather(both, axis, axis=0, tiled=True), 0, [])]
    all_gather x1 -> x0, waiting for transfers between devices: 47.7 us -> none  [on_device(): lax.all_gather(row_norm(middle, norm_gain), 'tp', axis=0, tiled=True)]
    ppermute x0 -> x3, waiting for transfers between devices: none -> 26.2 us  [the longest x2 26.2 us: ring_gather(): earlier.append(lax.ppermute(earlier[-1], axis, up))]
    reduce_scatter x1, waiting for transfers between devices: 37.5 us -> 46.6 us  [on_device(): lax.psum_scatter(down_sum.astype(jnp.bfloat16), 'tp', scatter_dimension=0...]
    unnamed x44 -> x55, local copies, waits for them, and re-layouts: 2.67 us -> 8.31 us
    all_gather x3, blocking collectives: 35.5 us -> 40.2 us  [gathered_once(): both, at, found = (lax.all_gather(jnp.concatenate(lines), axis), 0, {})]
  transfers between devices with their start and end apart: 4 -> 6, of which waited for: 4 -> 4; matrix products, arithmetic and copies ran while one was open for 0% -> 31% of each run, Pallas kernels for 0% -> 0%
where the time goes in v1:
time: 305 us; the launch traced here: 304 us
  waiting for transfers between devices  103 us (34%)
  local copies, waits for them, and re-layouts  57.5 us (19%)
  blocking collectives  40.2 us (13%)
  matrix products  36.1 us (12%)
  other arithmetic  26.8 us (9%)
  between operations  26.8 us (9%)
  starting transfers between devices  8.05 us (3%)
  loops' own time  4.56 us (1%)
    reduce_scatter x1, waiting for transfers between devices, on_device(): lax.psum_scatter(down_sum.astype(jnp.bfloat16), 'tp', scatter_dimension=0...  46.6 us
    all_gather x3, blocking collectives, gathered_once(): both, at, found = (lax.all_gather(jnp.concatenate(lines), axis), 0, {})  40.2 us
    all_to_all x1, waiting for transfers between devices, sum_at_owner(): lax.all_to_all(tiles, axis, split_axis=0, concat_axis=0, tiled=True)  30.6 us
    ppermute x2, waiting for transfers between devices, ring_gather(): earlier.append(lax.ppermute(earlier[-1], axis, up))  26.2 us
    dynamic_update_slice x18, local copies, waits for them, and re-layouts, local_group(): lax.scan(block_step, carried, (query_rot.reshape(blocks, BLOCK, count_of_...  21.1 us
    dot_general x1, matrix products, on_device(): down_sum = jnp.dot(hidden, down_full, preferred_element_type=jnp.float32)  20.8 us
    convert_element_type x28, local copies, waits for them, and re-layouts, entering(): part[k].astype(own.dtype)  11 us
    unnamed x55, local copies, waits for them, and re-layouts  8.31 us
  transfers between devices with their start and end apart: 6, of which 4 were waited for; matrix products, arithmetic and copies ran while one was open for 31% of the time, Pallas kernels for 0%

profile of v1, /device:TPU:1, one launch (start us, length us, event | category | flops | bytes accessed | tf_op | source)
XLA Modules:
  0.0 303.5 jit_solution(12342446104388072661)
XLA Ops:
  6.5 1.8 pad_maximum_fusion.2
  8.4 1.1 copy.156
  9.5 1.1 copy.158
  12.1 25.0 %while.27 = (s32[]{:T(128)}, f32[2,64,64]{2,1,0:T(8,128)S(1)}, f32[6,128,2,64]{1,0,3,2:T(8,128)}, f32[6,128,2]{2,1,0:T(8,128)S(1)}, f32[6,128,2,64]{1,0,3,2:T(8,...) while((s32[]{:T(128)}, f32[2,64,64]{2,1,0:T(8,128)S(1)}, ...), condition=%wide.region_5.6_spmd.clone, body=%wide.region_3.5_spmd.clone.sunk | while | flops 12877827 | bytes 1099440 | solution.py:145
  13.3 2.8 dynamic_update_slice.14
  17.4 2.8 dynamic_update_slice.14
  21.6 2.8 dynamic_update_slice.14
  25.7 2.8 dynamic_update_slice.14
  29.9 2.8 dynamic_update_slice.14
  34.1 2.8 dynamic_update_slice.14
  37.2 1.0 reshape_reshape.22
  44.4 1.0 bitcast_convert_fusion
  45.4 1.9 fusion.90
  47.4 0.9 maximum_multiply_fusion.1
  48.3 22.9 %while.26 = (s32[]{:T(128)}, f32[1,128,128]{2,1,0:T(8,128)S(1)}, f32[6,128,1,128]{3,1,0,2:T(8,128)}, f32[6,128,1]{1,2,0:T(1,128)S(1)}, f32[6,128,1,128]{3,2,1,0:...) while((s32[]{:T(128)}, f32[1,128,128]{2,1,0:T(8,128)S(1)}, ...), condition=%wide.region_2.3_spmd.clone, body=%wide.region_0.2_spmd.clone.sunk | while | flops 17006596 | bytes 1515172 | solution.py:145
  50.7 0.6 constant_dynamic-update-slice_fusion.10
  54.5 0.6 constant_dynamic-update-slice_fusion.10
  58.3 0.6 constant_dynamic-update-slice_fusion.10
  62.1 0.6 constant_dynamic-update-slice_fusion.10
  66.0 0.6 constant_dynamic-update-slice_fusion.10
  69.8 0.6 constant_dynamic-update-slice_fusion.10
  71.2 0.7 maximum_bitcast_fusion
  71.9 4.7 %all-gather.3 = bf16[2,194,128]{2,1,0:T(8,128)(2,1)S(1)} all-gather(bf16[1,194,128]{2,1,0:T(8,128)(2,1)S(1)} %maximum_bitcast_fusion), channel_id=2, replica_groups=mesh['sp_0'=8,'sp_1'=4,'sp_2'=2,'tp'=4] {'sp_2'}, dimensions={0}, use_global_device_ids=true | all-gather | bytes 148992 | tf_op jit(solution)/shard_map/all_gather | solution.py:55
  79.5 11.7 %all-gather.4 = bf16[4,194,128]{2,1,0:T(8,128)(2,1)S(1)} all-gather(bf16[1,194,128]{2,1,0:T(8,128)(2,1)S(1)} %maximum_bitcast_fusion.1), channel_id=3, replica_groups=mesh['sp_0'=8,'sp_1'=4,'sp_2'=2,'tp'=4] {'sp_1'}, dimensions={0}, use_global_device_ids=true | all-gather | bytes 248320 | tf_op jit(solution)/shard_map/all_gather | solution.py:55
  96.7 23.8 %all-gather.5 = bf16[8,194,128]{2,1,0:T(8,128)(2,1)S(1)} all-gather(bf16[1,194,128]{2,1,0:T(8,128)(2,1)S(1)} %maximum_bitcast_fusion.2), channel_id=4, replica_groups=mesh['sp_0'=8,'sp_1'=4,'sp_2'=2,'tp'=4] {'sp_0'}, dimensions={0}, use_global_device_ids=true | all-gather | bytes 446976 | tf_op jit(solution)/shard_map/all_gather | solution.py:55
  120.6 0.7 copy.173
  121.4 0.7 copy.174
  122.2 0.7 copy.175
  123.0 0.7 copy.176
  123.8 0.7 copy.177
  124.5 0.7 copy.178
  125.3 0.7 copy.179
  126.1 0.7 copy.180
  127.0 0.7 copy.181
  127.8 0.7 copy.182
  128.5 0.7 copy.183
  129.3 0.7 copy.184
  130.1 0.7 copy.185
  130.9 0.7 copy.186
  131.7 1.1 copy.170
  139.2 1.9 copy.169
  141.1 1.1 copy.153
  142.8 0.7 fusion.271
  143.5 1.5 fusion.295
  145.1 1.6 fusion.296
  147.0 1.0 fusion.95
  148.1 2.7 add_convert_fusion
  150.8 4.8 %all-to-all-start = ((bf16[4,192,2048]{2,1,0:T(8,128)(2,1)}), bf16[4,192,2048]{2,1,0:T(8,128)(2,1)}, u32[]{:S(2)}, u32[]{:S(2)}) async-start(bf16[4,192,2048]{2,1,0:T(8,128)(2,1)} %bitcast.453), calls=%async_computation | async-start | bytes 6291456 | tf_op jit(solution)/shard_map/all_to_all | solution.py:95
  155.8 30.6 %all-to-all-done = bf16[4,192,2048]{2,1,0:T(8,128)(2,1)} async-done(((bf16[4,192,2048]{2,1,0:T(8,128)(2,1)}), bf16[4,192,2048]{2,1,0:T(8,128)(2,1)}, u32[]{:S(2)}, u32[]{:S(2)}) %all-to-all-start) | async-done | bytes 3145760 | tf_op jit(solution)/shard_map/all_to_all | solution.py:95
  186.4 2.7 convert_reduce_fusion
  190.1 11.9 %collective-permute-done = bf16[192,2048]{1,0:T(8,128)(2,1)S(1)} collective-permute-done((bf16[192,2048]{1,0:T(8,128)(2,1)S(1)}, bf16[192,2048]{1,0:T(8,128)(2,1)S(1)}, u32[]{:S(2)}, u32[]{:S(2)}) %collective-permute-start) | collective-permute-done | bytes 786464 | tf_op jit(solution)/shard_map/ppermute | solution.py:23
  202.1 2.7 collective-permute-start.2
  204.8 14.2 %collective-permute-done.1 = bf16[192,2048]{1,0:T(8,128)(2,1)S(1)} collective-permute-done((bf16[192,2048]{1,0:T(8,128)(2,1)S(1)}, bf16[192,2048]{1,0:T(8,128)(2,1)S(1)}, u32[]{:S(2)}, u32[]{:S(2)}) %collective-permute-start.1) | collective-permute-done | bytes 786464 | tf_op jit(solution)/shard_map/ppermute | solution.py:23
  219.0 0.9 constant_dynamic-update-slice_fusion.8
  219.9 0.9 constant_dynamic-update-slice_fusion.7
  220.9 1.1 constant_dynamic-update-slice_fusion.6
  222.0 0.9 constant_dynamic-update-slice_fusion.5
  222.9 0.9 constant_dynamic-update-slice_fusion.4
  223.9 0.9 constant_dynamic-update-slice_fusion.3
  224.8 1.1 constant_dynamic-update-slice_fusion.2
  226.0 1.0 constant_dynamic-update-slice_fusion.1
  226.9 20.8 %fusion.55 = bf16[768,2048]{1,0:T(8,128)(2,1)} fusion(bf16[2048,4096]{1,0:T(8,128)(2,1)} %all-gather.8.cloned.1.call-done, bf16[1536,2048]{1,0:T(8,128)(2,1)} %constant_dynamic-update-slice_fusion.1, s32[]{:T(128)S(6)} %select_n.416), kind=kOutput, calls=%fused_computation.75 | convolution fusion | flops 12891193344 | bytes 23068676 | tf_op jit(solution)/shard_map/dot_general | solution.py:239
  247.8 46.6 %reduce-scatter.2.cloned.1.call-done = bf16[192,2048]{1,0:T(8,128)(2,1)} async-done(((bf16[768,2048]{1,0:T(8,128)(2,1)}), bf16[192,2048]{1,0:T(8,128)(2,1)}) %reduce-scatter.2.cloned.1.call-update) | async-done | bytes 786448 | tf_op jit(solution)/shard_map/reduce_scatter | solution.py:240
  294.4 2.3 fusion.66
  (305 shorter events, 36.0 us)
Async XLA Ops:
  6.5 140.5 %copy-start = (bf16[128,2048]{1,0:T(8,128)(2,1)S(1)}, bf16[128,2048]{1,0:T(8,128)(2,1)}, u32[]{:S(2)}) copy-start(bf16[128,2048]{1,0:T(8,128)(2,1)} %param.31) | copy-start | bytes 1572868
  6.5 4.7 %copy-start.6 = (bf16[768,128]{1,0:T(8,128)(2,1)S(1)}, bf16[768,128]{1,0:T(8,128)(2,1)}, u32[]{:S(2)}) copy-start(bf16[768,128]{1,0:T(8,128)(2,1)} %param.28) | copy-start | bytes 589828
  6.5 5.3 %copy-start.7 = (f32[2,768]{1,0:T(2,128)S(1)}, f32[2,768]{1,0:T(2,128)}, u32[]{:S(2)}) copy-start(f32[2,768]{1,0:T(2,128)} %param.30) | copy-start | bytes 18436
  6.5 220.4 %all-gather.8.cloned.1.call-start = ((), (), s32[]{:S(2)}) async-start(), calls=%async_computation.2 | async-start | bytes 17039360 | tf_op jit(solution)/shard_map/all_gather | solution.py:33
  11.3 26.9 %copy-start.16 = (f32[1,768]{1,0:T(1,128)S(1)}, f32[1,768]{1,0:T(1,128)}, u32[]{:S(2)}) copy-start(f32[1,768]{1,0:T(1,128)} %param.25) | copy-start | bytes 9220
  11.5 32.9 %copy-start.5 = (bf16[768,128]{1,0:T(8,128)(2,1)S(1)}, bf16[768,128]{1,0:T(8,128)(2,1)}, u32[]{:S(2)}) copy-start(bf16[768,128]{1,0:T(8,128)(2,1)} %param.21) | copy-start | bytes 589828
  38.9 0.5 copy-start.18
  71.2 60.4 %copy-start.4 = (f32[6,128,2,64]{1,0,3,2:T(8,128)S(1)}, f32[6,128,2,64]{1,0,3,2:T(8,128)}, u32[]{:S(2)}) copy-start(f32[6,128,2,64]{1,0,3,2:T(8,128)} %get-tuple-element.84) | copy-start | bytes 1179652
  77.8 13.4 %copy-start.10 = (f32[2]{0:T(128)}, f32[2]{0:T(128)S(1)}, u32[]{:S(2)}) copy-start(f32[2]{0:T(128)S(1)} %get-tuple-element.262) | copy-start | bytes 28
  78.0 1.5 copy-start.17
  94.9 1.7 copy-start.8
  95.0 0.6 copy-start.14
  95.1 1.5 copy-start.12
  95.1 1.5 copy-start.13
  96.7 48.4 %copy-start.9 = (f32[2]{0:T(128)S(1)}, f32[2]{0:T(128)}, u32[]{:S(2)}) copy-start(f32[2]{0:T(128)} %copy-done.8) | copy-start | bytes 28
  126.9 18.2 %copy-start.11 = (f32[2]{0:T(128)S(1)}, f32[2]{0:T(128)}, u32[]{:S(2)}) copy-start(f32[2]{0:T(128)} %copy-done.10) | copy-start | bytes 28
  146.9 1.2 copy-start.3
  148.1 7.7 %copy-start.15 = (bf16[2048]{0:T(1024)(128)(2,1)S(1)}, bf16[2048]{0:T(1024)(128)(2,1)}, u32[]{:S(2)}) copy-start(bf16[2048]{0:T(1024)(128)(2,1)} %param.33) | copy-start | bytes 12292
  150.8 38.4 %copy-start.1 = (bf16[192,2048]{1,0:T(8,128)(2,1)S(1)}, bf16[192,2048]{1,0:T(8,128)(2,1)}, u32[]{:S(2)}) copy-start(bf16[192,2048]{1,0:T(8,128)(2,1)} %param.20) | copy-start | bytes 2359300
  150.8 35.7 %all-to-all-start = ((bf16[4,192,2048]{2,1,0:T(8,128)(2,1)}), bf16[4,192,2048]{2,1,0:T(8,128)(2,1)}, u32[]{:S(2)}, u32[]{:S(2)}) async-start(bf16[4,192,2048]{2,1,0:T(8,128)(2,1)} %bitcast.453), calls=%async_computation | async-start | bytes 6291456 | tf_op jit(solution)/shard_map/all_to_all | solution.py:95
  155.6 138.8 %reduce-scatter.2.cloned.1.call-start = ((), (), s32[]{:S(2)}) async-start(), calls=%async_computation.3 | async-start | bytes 3932160 | tf_op jit(solution)/shard_map/reduce_scatter | solution.py:240
  189.8 12.3 %copy-start.2 = (bf16[192,2048]{1,0:T(8,128)(2,1)}, bf16[192,2048]{1,0:T(8,128)(2,1)S(1)}, u32[]{:S(2)}) copy-start(bf16[192,2048]{1,0:T(8,128)(2,1)S(1)} %fusion.65) | copy-start | bytes 2359300
  189.8 12.3 %collective-permute-start = (bf16[192,2048]{1,0:T(8,128)(2,1)S(1)}, bf16[192,2048]{1,0:T(8,128)(2,1)S(1)}, u32[]{:S(2)}, u32[]{:S(2)}) collective-permute-start(bf16[192,2048]{1,0:T(8,128)(2,1)S(1)} %fusion.65), channel_id=1, source_target_pairs={{0,1},{1,2},{2,3},{3,0},{4,5},{5,6},{6,7},{7,4},{8,9},{9,10},{10,1... | collective-permute-start | bytes 2359304 | tf_op jit(solution)/shard_map/ppermute | solution.py:23
  202.1 16.9 %collective-permute-start.1 = (bf16[192,2048]{1,0:T(8,128)(2,1)S(1)}, bf16[192,2048]{1,0:T(8,128)(2,1)S(1)}, u32[]{:S(2)}, u32[]{:S(2)}) collective-permute-start(bf16[192,2048]{1,0:T(8,128)(2,1)S(1)} %collective-permute-done), channel_id=1, source_target_pairs={{0,1},{1,2},{2,3},{3,0},{4,5},{5,6},{6,7},{7,4},{8,9},{9,10},{10,1... | collective-permute-start | bytes 2359304 | tf_op jit(solution)/shard_map/ppermute | solution.py:23
  202.1 19.9 %collective-permute-start.2 = (bf16[192,2048]{1,0:T(8,128)(2,1)}, bf16[192,2048]{1,0:T(8,128)(2,1)S(1)}, u32[]{:S(2)}, u32[]{:S(2)}) collective-permute-start(bf16[192,2048]{1,0:T(8,128)(2,1)} %copy-done.2), channel_id=1, source_target_pairs={{0,3},{1,0},{2,1},{3,2},{4,7},{5,4},{6,5},{7,6},{8,11},{9,8},{10,9... | collective-permute-start | bytes 2359304 | tf_op jit(solution)/shard_map/ppermute | solution.py:25
Sparse Core Ops, SparseCore 0:
  10.1 106.7 all-gather.7
  247.9 46.4 reduce-scatter.1
